TPU v7x, 32 devices: a whole 2x2x4 slice. The times are simulated.
32 devices in a mesh: kv: 8 (over z, y), tp: 4 (over x, core).
Axes of the slice: x: 2, y: 2, z: 4, core: 2. Of those that a mesh axis runs over, the one named last changes fastest.
Arguments:
- x_piece: bfloat16 [128, 2048], P('kv'), may hold values from -6 to 6
- x_decode: bfloat16 [8, 2048], P('kv'), may hold values from -6 to 6
- norm_gain: float32 [2048], replicated, may hold values from 0.1 to 1.9
- w_query: bfloat16 [2048, 1024], P(None, 'tp'), may hold values from -0.1875 to 0.1875
- w_key: bfloat16 [2048, 1024], P(None, 'tp'), may hold values from -0.1875 to 0.1875
- w_value: bfloat16 [2048, 1024], P(None, 'tp'), may hold values from -0.125 to 0.125
- w_out: bfloat16 [1024, 2048], P(None, 'tp'), may hold values from -0.1875 to 0.1875
- head_gain: float32 [128], replicated, may hold values from 0.1 to 1.9
- lambdas: float32 [8], P('tp'), may hold values from 0.3 to 0.8
- piece_keys: bfloat16 [4096, 8, 128], P('kv', 'tp'), may hold values from -300 to 300
- piece_values: bfloat16 [4096, 8, 128], P('kv', 'tp'), may hold values from -6 to 6
- cache_keys: bfloat16 [8, 2048, 8, 128], P('kv', None, 'tp'), may hold values from -300 to 300
- cache_values: bfloat16 [8, 2048, 8, 128], P('kv', None, 'tp'), may hold values from -6 to 6
- cache_lengths: int32 [8], P('kv'), may hold values from 1 to 2048, as said below
Outputs:
- piece_out: bfloat16 [128, 2048], P('kv', 'tp')
- decode_out: bfloat16 [8, 2048], P('kv', 'tp')
Inputs may be any that keep to these rules, and one draw needn't show every extreme that they name: `cache_lengths`: some sequence has exactly 2048 filled slots.
All inputs are finite; a program needn't handle non-finite values.
Results may differ from a plain program's by a relative error of at most 0.013.
The roundings to bfloat16 on the way count: a program that leaves them out, or rounds other values in their place, can miss the bound.
Values may be sent and summed in bfloat16 or wider, within the bound.
A program may use at most 64 MiB of HBM per device.

v0:
```python
import math

import jax
import jax.numpy as jnp
from jax import lax
from jax.sharding import PartitionSpec as P

EPS = 1e-06


def shards(
    x_piece,
    x_decode,
    norm_gain,
    w_query,
    w_key,
    w_value,
    w_out,
    head_gain,
    lambdas,
    piece_keys,
    piece_values,
    cache_keys,
    cache_values,
    cache_lengths,
):
    piece_rows = x_piece.shape[0]
    local_heads = lambdas.shape[0]
    pair_width = piece_keys.shape[2]
    half_width = pair_width // 2
    value_width = piece_values.shape[2]
    score_scale = 1.0 / math.sqrt(half_width)
    cached = piece_keys.shape[0]
    all_rows = jnp.concatenate([x_piece, x_decode], axis=0)
    row_count = all_rows.shape[0]
    rows32 = all_rows.astype(jnp.float32)
    normed = (
        rows32 * lax.rsqrt(jnp.mean(rows32 * rows32, axis=-1, keepdims=True) + EPS) * norm_gain
    ).astype(jnp.bfloat16)
    queries = (
        jnp.dot(normed, w_query, preferred_element_type=jnp.float32)
        .astype(jnp.bfloat16)
        .reshape(row_count, local_heads, pair_width)
    )
    new_keys = (
        jnp.dot(normed, w_key, preferred_element_type=jnp.float32)
        .astype(jnp.bfloat16)
        .reshape(row_count, local_heads, pair_width)
    )
    new_values = (
        jnp.dot(normed, w_value, preferred_element_type=jnp.float32)
        .astype(jnp.bfloat16)
        .reshape(row_count, local_heads, value_width)
    )
    keys_all = jnp.concatenate([piece_keys, new_keys[:piece_rows]], axis=0)
    values_all = jnp.concatenate([piece_values, new_values[:piece_rows]], axis=0)
    offset = lax.axis_index("kv") * piece_rows
    kv_count = lax.axis_size("kv")
    total_rows = piece_rows * kv_count
    key_index = jnp.arange(cached + piece_rows, dtype=jnp.int32)

    def block_terms(query_block, block_start):
        block_rows = query_block.shape[0]
        query_pos = block_start + jnp.arange(block_rows, dtype=jnp.int32)
        allowed = (key_index[None, :] < cached) | (
            key_index[None, :] - cached + offset <= query_pos[:, None]
        )
        results = []
        for which_map in range(2):
            lower = which_map * half_width
            scores = (
                jnp.einsum(
                    "qhd,khd->hqk",
                    query_block[:, :, lower : lower + half_width],
                    keys_all[:, :, lower : lower + half_width],
                    preferred_element_type=jnp.float32,
                )
                * score_scale
            )
            scores = jnp.where(allowed[None], scores, -jnp.inf)
            row_max = jnp.max(scores, axis=-1)
            weights = jnp.exp(scores - row_max[..., None])
            totals = jnp.sum(weights, axis=-1)
            mixed = jnp.einsum(
                "hqk,khd->qhd",
                weights.astype(jnp.bfloat16),
                values_all,
                preferred_element_type=jnp.float32,
            )
            results += [row_max, totals, mixed.reshape(block_rows, local_heads * value_width)]
        return tuple(results)

    stat_zeros = jnp.zeros((local_heads, total_rows), jnp.float32)
    value_zeros = jnp.zeros((total_rows, local_heads * value_width), jnp.float32)
    initial = (stat_zeros, stat_zeros, value_zeros, stat_zeros, stat_zeros, value_zeros)
    piece = lax.all_gather(queries[:piece_rows], "kv", axis=0, tiled=True)
    start = jnp.int32(0)
    block_rows = piece.shape[0]
    if block_rows > 512 and block_rows % 512 == 0:
        nblocks = block_rows // 512
        blocks = piece.reshape(nblocks, 512, local_heads, pair_width)
        starts = start + 512 * jnp.arange(nblocks, dtype=jnp.int32)
        mapped = lax.map(lambda inputs: block_terms(inputs[0], inputs[1]), (blocks, starts))
        results = []
        for index, entry in enumerate(mapped):
            if index % 3 == 2:
                results.append(entry.reshape(block_rows, local_heads * value_width))
            else:
                results.append(entry.transpose(1, 0, 2).reshape(local_heads, block_rows))
        results = tuple(results)
    else:
        results = block_terms(piece, start)
    updated = []
    for index in range(6):
        along = 0 if index % 3 == 2 else 1
        updated.append(
            lax.dynamic_update_slice_in_dim(initial[index], results[index], start, along)
        )
    partials = tuple(updated)
    moved_values = (
        lax.all_to_all(
            partials[2].astype(jnp.bfloat16), "kv", split_axis=0, concat_axis=0, tiled=True
        ).astype(jnp.float32),
        lax.all_to_all(
            partials[5].astype(jnp.bfloat16), "kv", split_axis=0, concat_axis=0, tiled=True
        ).astype(jnp.float32),
    )
    moved_stats = (
        lax.all_to_all(partials[0], "kv", split_axis=1, concat_axis=1, tiled=True),
        lax.all_to_all(partials[1], "kv", split_axis=1, concat_axis=1, tiled=True),
        lax.all_to_all(partials[3], "kv", split_axis=1, concat_axis=1, tiled=True),
        lax.all_to_all(partials[4], "kv", split_axis=1, concat_axis=1, tiled=True),
    )
    own = []
    for which_map in range(2):
        maxima = moved_stats[2 * which_map].reshape(local_heads, kv_count, piece_rows)
        sums = moved_stats[2 * which_map + 1].reshape(local_heads, kv_count, piece_rows)
        weighted = moved_values[which_map].reshape(kv_count, piece_rows, local_heads * value_width)
        new_max = jnp.max(maxima, axis=1)
        factor = jnp.exp(maxima - new_max[:, None, :])
        value_factor = jnp.repeat(factor.transpose(1, 2, 0), value_width, axis=2)
        own += [new_max, jnp.sum(factor * sums, axis=1), jnp.sum(value_factor * weighted, axis=0)]
    lambda_wide = jnp.repeat(lambdas, value_width)[None, :]
    piece_mixed = own[2] / jnp.repeat(own[1].T, value_width, axis=1) - lambda_wide * own[
        5
    ] / jnp.repeat(own[4].T, value_width, axis=1)
    dec_query = queries[piece_rows:]
    own_keys = new_keys[piece_rows:]
    own_values = new_values[piece_rows:].astype(jnp.float32)
    slot_index = jnp.arange(cache_keys.shape[1], dtype=jnp.int32)
    slot_allowed = slot_index[None, None, :] < cache_lengths[:, None, None]
    dec_results = []
    for which_map in range(2):
        lower = which_map * half_width
        scores = (
            jnp.einsum(
                "bhd,bkhd->bhk",
                dec_query[:, :, lower : lower + half_width],
                cache_keys[:, :, :, lower : lower + half_width],
                preferred_element_type=jnp.float32,
            )
            * score_scale
        )
        scores = jnp.where(slot_allowed, scores, -jnp.inf)
        own_score = (
            jnp.einsum(
                "bhd,bhd->bh",
                dec_query[:, :, lower : lower + half_width],
                own_keys[:, :, lower : lower + half_width],
                preferred_element_type=jnp.float32,
            )
            * score_scale
        )
        row_max = jnp.maximum(jnp.max(scores, axis=-1), own_score)
        weights = jnp.exp(scores - row_max[..., None])
        own_weight = jnp.exp(own_score - row_max)
        totals = jnp.sum(weights, axis=-1) + own_weight
        mixed = jnp.einsum(
            "bhk,bkhd->bhd",
            weights.astype(jnp.bfloat16),
            cache_values,
            preferred_element_type=jnp.float32,
        )
        mixed = mixed + own_weight.astype(jnp.bfloat16).astype(jnp.float32)[..., None] * own_values
        dec_results.append(mixed / totals[..., None])
    dec_mixed = (dec_results[0] - lambdas[None, :, None] * dec_results[1]).reshape(
        -1, local_heads * value_width
    )
    attended = jnp.concatenate([piece_mixed, dec_mixed], axis=0).reshape(
        row_count, local_heads, value_width
    )
    head_out = (
        attended
        * lax.rsqrt(jnp.mean(attended * attended, axis=-1, keepdims=True) + EPS)
        * head_gain
    ).astype(jnp.bfloat16)
    head_out = head_out.reshape(row_count, local_heads * value_width)
    output = jnp.dot(
        lax.all_gather(head_out, "tp", axis=1, tiled=True),
        w_out,
        preferred_element_type=jnp.float32,
    )
    output = output.astype(jnp.bfloat16)
    return (output[:piece_rows], output[piece_rows:])


def solution(mesh):
    placed = (
        P("kv", None),
        P("kv", None),
        P(),
        P(None, "tp"),
        P(None, "tp"),
        P(None, "tp"),
        P(None, "tp"),
        P(),
        P("tp"),
        P("kv", "tp", None),
        P("kv", "tp", None),
        P("kv", None, "tp", None),
        P("kv", None, "tp", None),
        P("kv"),
    )
    return jax.shard_map(
        shards,
        mesh=mesh,
        in_specs=placed,
        out_specs=(P("kv", "tp"), P("kv", "tp")),
        check_vma=False,
    )
```

profile of v0, /device:TPU:0, one launch (start us, length us, event | category | flops | bytes accessed | tf_op | source)
XLA Modules:
  0.0 112.1 jit_solution(12364098062893879880)
XLA Ops:
  0.7 1.1 %fusion.21 = f32[17]{0:T(128)S(1)} fusion(bf16[1,2048]{1,0:T(2,128)(2,1)} %param.15, bf16[16,2048]{1,0:T(8,128)(2,1)} %param.14), kind=kLoop, calls=%fused_computation.37 | loop fusion | flops 208879 | bytes 69700 | tf_op jit(solution)/shard_map/reduce_sum | solution.py:38
  1.9 1.6 %convolution_convert_fusion.5 = bf16[17,256]{1,0:T(8,128)(2,1)S(1)} fusion(bf16[2048,256]{1,0:T(8,128)(2,1)} %param.17, f32[2048]{0:T(1024)} %param.16, f32[17]{0:T(128)S(1)} %add_rsqrt_fusion.1, bf16[1,2048]{1,0:T(2,128)(2,1)} %param.15, bf16[16,2048]{1,0:T(8,128)(2,1)S(1)} %copy-done.2), kind=kOutput, calls=%fused_computation.11 | convolution fusion | flops 18073856 | bytes 1135172 | tf_op jit(solution)/shard_map/dot_general | solution.py:41
  3.8 32.5 %all_gather.6 = bf16[128,2,128]{2,1,0:T(2,128)(2,1)S(1)} all-gather(bf16[16,2,128]{2,1,0:T(2,128)(2,1)S(1)} %slice.73), channel_id=1, replica_groups=mesh['kv'=8,'tp'=4] {'kv'}, dimensions={0}, use_global_device_ids=true | all-gather | bytes 73728 | tf_op jit(solution)/shard_map/all_gather | solution.py:96
  37.4 0.6 copy.77
  38.0 5.5 %all-to-all-start.5 = ((f32[2,8,16]{2,0,1:T(2,128)}), f32[2,8,16]{2,0,1:T(2,128)S(1)}, u32[]{:S(2)}, u32[]{:S(2)}) async-start(f32[2,8,16]{2,0,1:T(2,128)} %copy.77), calls=%async_computation.5 | async-start | bytes 16384 | tf_op jit(solution)/shard_map/all_to_all | solution.py:132
  43.7 1.9 %slice_bitcast_fusion = (bf16[2048,2,64]{2,1,0:T(2,128)(2,1)S(1)}, bf16[2048,2,64]{2,1,0:T(2,128)(2,1)S(1)}) fusion(bf16[1,2048,2,128]{3,2,1,0:T(2,128)(2,1)S(1)} %copy-done.1), kind=kLoop, calls=%fused_computation.16 | loop fusion | bytes 2097152 | tf_op jit(solution)/shard_map/reshape.43
  46.4 0.4 fusion.4
  46.8 0.4 fusion.6
  48.1 0.7 copy-done.4
  49.1 0.6 copy-done.7
  49.8 0.3 fusion.3
  50.2 0.3 fusion.59
  50.5 0.3 fusion.2
  50.8 0.6 copy-done.10
  51.6 0.6 copy.74
  52.2 6.1 %all-to-all-start.3 = ((f32[2,8,16]{2,0,1:T(2,128)}), f32[2,8,16]{2,0,1:T(2,128)S(1)}, u32[]{:S(2)}, u32[]{:S(2)}) async-start(f32[2,8,16]{2,0,1:T(2,128)} %copy.74), calls=%async_computation.3 | async-start | bytes 16384 | tf_op jit(solution)/shard_map/all_to_all | solution.py:131
  58.5 0.6 copy.65
  59.1 5.8 %all-to-all-done.3 = f32[2,8,16]{2,0,1:T(2,128)S(1)} async-done(((f32[2,8,16]{2,0,1:T(2,128)}), f32[2,8,16]{2,0,1:T(2,128)S(1)}, u32[]{:S(2)}, u32[]{:S(2)}) %all-to-all-start.3) | async-done | bytes 1056 | tf_op jit(solution)/shard_map/all_to_all | solution.py:131
  64.9 3.3 %all-to-all-start = ((f32[2,8,16]{2,0,1:T(2,128)}), f32[2,8,16]{2,0,1:T(2,128)S(1)}, u32[]{:S(2)}, u32[]{:S(2)}) async-start(f32[2,8,16]{2,0,1:T(2,128)} %copy.65), calls=%async_computation | async-start | bytes 16384 | tf_op jit(solution)/shard_map/all_to_all | solution.py:129
  68.4 0.7 convert_element_type.100
  69.2 0.6 copy.70
  69.9 0.7 convert_element_type.95
  70.6 4.1 %all-to-all-done = f32[2,8,16]{2,0,1:T(2,128)S(1)} async-done(((f32[2,8,16]{2,0,1:T(2,128)}), f32[2,8,16]{2,0,1:T(2,128)S(1)}, u32[]{:S(2)}, u32[]{:S(2)}) %all-to-all-start) | async-done | bytes 1056 | tf_op jit(solution)/shard_map/all_to_all | solution.py:129
  74.7 3.3 %all-to-all-start.2 = ((f32[2,8,16]{2,0,1:T(2,128)}), f32[2,8,16]{2,0,1:T(2,128)S(1)}, u32[]{:S(2)}, u32[]{:S(2)}) async-start(f32[2,8,16]{2,0,1:T(2,128)} %copy.70), calls=%async_computation.2 | async-start | bytes 16384 | tf_op jit(solution)/shard_map/all_to_all | solution.py:130
  78.5 6.0 %all-to-all-done.2 = f32[2,8,16]{2,0,1:T(2,128)S(1)} async-done(((f32[2,8,16]{2,0,1:T(2,128)}), f32[2,8,16]{2,0,1:T(2,128)S(1)}, u32[]{:S(2)}, u32[]{:S(2)}) %all-to-all-start.2) | async-done | bytes 1056 | tf_op jit(solution)/shard_map/all_to_all | solution.py:130
  84.5 3.3 %all-to-all-start.4 = ((bf16[8,16,256]{2,1,0:T(8,128)(2,1)}), bf16[8,16,256]{2,1,0:T(8,128)(2,1)S(1)}, u32[]{:S(2)}, u32[]{:S(2)}) async-start(bf16[8,16,256]{2,1,0:T(8,128)(2,1)} %convert_element_type.100), calls=%async_computation.4 | async-start | bytes 131072 | tf_op jit(solution)/shard_map/all_to_all | solution.py:124
  88.5 6.2 %all-to-all-done.4 = bf16[8,16,256]{2,1,0:T(8,128)(2,1)S(1)} async-done(((bf16[8,16,256]{2,1,0:T(8,128)(2,1)}), bf16[8,16,256]{2,1,0:T(8,128)(2,1)S(1)}, u32[]{:S(2)}, u32[]{:S(2)}) %all-to-all-start.4) | async-done | bytes 65568 | tf_op jit(solution)/shard_map/all_to_all | solution.py:124
  94.7 3.3 %all-to-all-start.1 = ((bf16[8,16,256]{2,1,0:T(8,128)(2,1)}), bf16[8,16,256]{2,1,0:T(8,128)(2,1)S(1)}, u32[]{:S(2)}, u32[]{:S(2)}) async-start(bf16[8,16,256]{2,1,0:T(8,128)(2,1)} %convert_element_type.95), calls=%async_computation.1 | async-start | bytes 131072 | tf_op jit(solution)/shard_map/all_to_all | solution.py:121
  98.1 6.8 %all-to-all-done.1 = bf16[8,16,256]{2,1,0:T(8,128)(2,1)S(1)} async-done(((bf16[8,16,256]{2,1,0:T(8,128)(2,1)}), bf16[8,16,256]{2,1,0:T(8,128)(2,1)S(1)}, u32[]{:S(2)}, u32[]{:S(2)}) %all-to-all-start.1) | async-done | bytes 65568 | tf_op jit(solution)/shard_map/all_to_all | solution.py:121
  105.5 5.2 %all_gather.7 = bf16[17,1024]{1,0:T(8,128)(2,1)S(1)} all-gather(bf16[17,256]{1,0:T(8,128)(2,1)S(1)} %fusion.30), channel_id=1, replica_groups=mesh['kv'=8,'tp'=4] {'tp'}, dimensions={1}, use_global_device_ids=true | all-gather | bytes 43520 | tf_op jit(solution)/shard_map/all_gather | solution.py:199
  110.9 0.6 slice.105
  111.5 0.6 slice.106
  (87 shorter events, 5.7 us)
Async XLA Ops:
  0.6 47.0 %copy-start = (bf16[1,2048,2,128]{3,2,1,0:T(2,128)(2,1)S(1)}, bf16[1,2048,2,128]{3,2,1,0:T(2,128)(2,1)}, u32[]{:S(2)}) copy-start(bf16[1,2048,2,128]{3,2,1,0:T(2,128)(2,1)} %param.26) | copy-start | bytes 3145732
  0.6 1.2 %copy-start.2 = (bf16[16,2048]{1,0:T(8,128)(2,1)S(1)}, bf16[16,2048]{1,0:T(8,128)(2,1)}, u32[]{:S(2)}) copy-start(bf16[16,2048]{1,0:T(8,128)(2,1)} %param.14) | copy-start | bytes 196612
  0.7 2.8 %copy-start.3 = (bf16[2048,256]{1,0:T(8,128)(2,1)S(1)}, bf16[2048,256]{1,0:T(8,128)(2,1)}, u32[]{:S(2)}) copy-start(bf16[2048,256]{1,0:T(8,128)(2,1)} %param.18) | copy-start | bytes 3145732
  1.8 1.6 %copy-start.8 = (bf16[1,2048]{1,0:T(2,128)(2,1)S(1)}, bf16[1,2048]{1,0:T(2,128)(2,1)}, u32[]{:S(2)}) copy-start(bf16[1,2048]{1,0:T(2,128)(2,1)} %param.15) | copy-start | bytes 12292
  1.8 1.6 %copy-start.9 = (f32[2048]{0:T(1024)S(1)}, f32[2048]{0:T(1024)}, u32[]{:S(2)}) copy-start(f32[2048]{0:T(1024)} %param.16) | copy-start | bytes 24580
  3.8 32.8 %copy-start.6 = (bf16[512,2,128]{2,1,0:T(2,128)(2,1)S(1)}, bf16[512,2,128]{2,1,0:T(2,128)(2,1)}, u32[]{:S(2)}) copy-start(bf16[512,2,128]{2,1,0:T(2,128)(2,1)} %param.23) | copy-start | bytes 786436
  36.5 7.1 %copy-start.1 = (bf16[1,2048,2,128]{3,2,1,0:T(2,128)(2,1)S(1)}, bf16[1,2048,2,128]{3,2,1,0:T(2,128)(2,1)}, u32[]{:S(2)}) copy-start(bf16[1,2048,2,128]{3,2,1,0:T(2,128)(2,1)} %param.25) | copy-start | bytes 3145732
  38.0 14.2 %all-to-all-start.5 = ((f32[2,8,16]{2,0,1:T(2,128)}), f32[2,8,16]{2,0,1:T(2,128)S(1)}, u32[]{:S(2)}, u32[]{:S(2)}) async-start(f32[2,8,16]{2,0,1:T(2,128)} %copy.77), calls=%async_computation.5 | async-start | bytes 16384 | tf_op jit(solution)/shard_map/all_to_all | solution.py:132
  47.6 1.2 %copy-start.4 = (bf16[2048,256]{1,0:T(8,128)(2,1)S(1)}, bf16[2048,256]{1,0:T(8,128)(2,1)}, u32[]{:S(2)}) copy-start(bf16[2048,256]{1,0:T(8,128)(2,1)} %param.19) | copy-start | bytes 3145732
  48.8 0.9 copy-start.7
  50.8 0.7 copy-start.10
  52.2 6.1 %copy-start.11 = (f32[128]{0:T(128)S(1)}, f32[128]{0:T(128)}, u32[]{:S(2)}) copy-start(f32[128]{0:T(128)} %param.21) | copy-start | bytes 1540
  52.2 12.7 %all-to-all-start.3 = ((f32[2,8,16]{2,0,1:T(2,128)}), f32[2,8,16]{2,0,1:T(2,128)S(1)}, u32[]{:S(2)}, u32[]{:S(2)}) async-start(f32[2,8,16]{2,0,1:T(2,128)} %copy.74), calls=%async_computation.3 | async-start | bytes 16384 | tf_op jit(solution)/shard_map/all_to_all | solution.py:131
  64.9 9.8 %all-to-all-start = ((f32[2,8,16]{2,0,1:T(2,128)}), f32[2,8,16]{2,0,1:T(2,128)S(1)}, u32[]{:S(2)}, u32[]{:S(2)}) async-start(f32[2,8,16]{2,0,1:T(2,128)} %copy.65), calls=%async_computation | async-start | bytes 16384 | tf_op jit(solution)/shard_map/all_to_all | solution.py:129
  74.7 9.8 %all-to-all-start.2 = ((f32[2,8,16]{2,0,1:T(2,128)}), f32[2,8,16]{2,0,1:T(2,128)S(1)}, u32[]{:S(2)}, u32[]{:S(2)}) async-start(f32[2,8,16]{2,0,1:T(2,128)} %copy.70), calls=%async_computation.2 | async-start | bytes 16384 | tf_op jit(solution)/shard_map/all_to_all | solution.py:130
  78.4 32.3 %copy-start.5 = (bf16[1024,512]{1,0:T(8,128)(2,1)S(1)}, bf16[1024,512]{1,0:T(8,128)(2,1)}, u32[]{:S(2)}) copy-start(bf16[1024,512]{1,0:T(8,128)(2,1)} %param.20) | copy-start | bytes 3145732
  84.5 10.2 %all-to-all-start.4 = ((bf16[8,16,256]{2,1,0:T(8,128)(2,1)}), bf16[8,16,256]{2,1,0:T(8,128)(2,1)S(1)}, u32[]{:S(2)}, u32[]{:S(2)}) async-start(bf16[8,16,256]{2,1,0:T(8,128)(2,1)} %convert_element_type.100), calls=%async_computation.4 | async-start | bytes 131072 | tf_op jit(solution)/shard_map/all_to_all | solution.py:124
  94.7 10.2 %all-to-all-start.1 = ((bf16[8,16,256]{2,1,0:T(8,128)(2,1)}), bf16[8,16,256]{2,1,0:T(8,128)(2,1)S(1)}, u32[]{:S(2)}, u32[]{:S(2)}) async-start(bf16[8,16,256]{2,1,0:T(8,128)(2,1)} %convert_element_type.95), calls=%async_computation.1 | async-start | bytes 131072 | tf_op jit(solution)/shard_map/all_to_all | solution.py:121
where the time goes:
time: 113 us; the launch traced here: 112 us
  blocking collectives  37.7 us (33%)
  waiting for transfers between devices  28.8 us (25%)
  starting transfers between devices  25 us (22%)
  local copies, waits for them, and re-layouts  11.4 us (10%)
  matrix products  4.9 us (4%)
  other arithmetic  2.63 us (2%)
  between operations  1.7 us (2%)
    all_gather x1, blocking collectives, shards(): piece = lax.all_gather(queries[:piece_rows], 'kv', axis=0, tiled=True)  32.5 us
    all_to_all x1, waiting for transfers between devices, shards(): lax.all_to_all(partials[2].astype(jnp.bfloat16), 'kv', split_axis=0, conc...  6.8 us
    all_to_all x1, waiting for transfers between devices, shards(): lax.all_to_all(partials[5].astype(jnp.bfloat16), 'kv', split_axis=0, conc...  6.2 us
    all_to_all x1, starting transfers between devices, shards(): lax.all_to_all(partials[3], 'kv', split_axis=1, concat_axis=1, tiled=True)  6.13 us
    all_to_all x1, waiting for transfers between devices, shards(): lax.all_to_all(partials[1], 'kv', split_axis=1, concat_axis=1, tiled=True)  5.96 us
    all_to_all x1, waiting for transfers between devices, shards(): lax.all_to_all(partials[3], 'kv', split_axis=1, concat_axis=1, tiled=True)  5.82 us
    all_to_all x1, starting transfers between devices, shards(): lax.all_to_all(partials[4], 'kv', split_axis=1, concat_axis=1, tiled=True)  5.49 us
    all_gather x1, blocking collectives, shards(): lax.all_gather(head_out, 'tp', axis=1, tiled=True)  5.22 us
  transfers between devices with their start and end apart: 6, of which 5 were waited for; matrix products, arithmetic and copies ran while one was open for 9% of the time, Pallas kernels for 0%

commit v1 on v0

v1 whole, which is shorter than its diff:
```python
import functools
import math

import jax
import jax.numpy as jnp
from jax import lax
from jax.experimental import pallas as pl
from jax.experimental.pallas import tpu as pltpu
from jax.sharding import PartitionSpec as P

EPS = 1e-06
MESH = pl.DeviceIdType.MESH
F32 = jnp.float32
BF16 = jnp.bfloat16
PAD = 16
LANES = 128
NEG = -jnp.inf


def dot_t(a, b):
    return lax.dot_general(a, b, (((1,), (1,)), ((), ())), preferred_element_type=F32)


def iota(shape, axis):
    return lax.broadcasted_iota(jnp.int32, shape, axis)


def step_kernel(
    kv, tp, rows, seqs, heads, width, group,
    xp, xd, ng, wq, wk, wv, wo, hg, lam, pk, pv, ck, cv, ln,
    po, do,
    xp_v, wq_v, wk_v, wv_v, wo_v, pk_v, pv_v, ck_v, cv_v,
    nrm, kf, vf, kh, vh, knew, vnew, qbuf, sbuf, rbuf, hbuf,
    load_sem, q_send, q_recv, s_send, s_recv, d_send, d_recv, h_send, h_recv,
):
    half = width // 2
    hw = heads * width
    maps = 2 * heads
    scale = math.log2(math.e) / math.sqrt(half)
    me = lax.axis_index("kv")
    col = lax.axis_index("tp")
    total = rows + PAD * seqs
    cached = kh.shape[1]

    pairs = [
        (xp, xp_v), (wq, wq_v), (wk, wk_v), (wv, wv_v), (ck, ck_v), (cv, cv_v),
        (pk, pk_v), (pv, pv_v), (wo, wo_v),
    ]
    loads = [pltpu.make_async_copy(s, d, load_sem.at[i]) for i, (s, d) in enumerate(pairs)]
    for load in loads:
        load.start()
    l_xp, l_wq, l_wk, l_wv, l_ck, l_cv, l_pk, l_pv, l_wo = loads

    def kv_peer(d):
        return {"kv": lax.rem(me + d, kv)}

    def tp_peer(d):
        return {"tp": lax.rem(col + d, tp)}

    barrier = pltpu.get_barrier_semaphore()
    for d in range(1, kv):
        pl.semaphore_signal(barrier, inc=1, device_id=kv_peer(d), device_id_type=MESH)
    for d in range(1, tp):
        pl.semaphore_signal(barrier, inc=1, device_id=tp_peer(d), device_id_type=MESH)

    def q_copy(d):
        return pltpu.make_async_remote_copy(
            src_ref=qbuf.at[0], dst_ref=qbuf.at[kv - d],
            send_sem=q_send.at[d], recv_sem=q_recv.at[kv - d],
            device_id=kv_peer(d), device_id_type=MESH,
        )

    def s_copy(d):
        return pltpu.make_async_remote_copy(
            src_ref=sbuf.at[d], dst_ref=rbuf.at[kv - d],
            send_sem=s_send.at[d], recv_sem=s_recv.at[kv - d],
            device_id=kv_peer(d), device_id_type=MESH,
        )

    def h_copy(d, start, size, send, recv):
        return pltpu.make_async_remote_copy(
            src_ref=hbuf.at[0, pl.ds(start, size)], dst_ref=hbuf.at[tp - d, pl.ds(start, size)],
            send_sem=send.at[d], recv_sem=recv.at[tp - d],
            device_id=tp_peer(d), device_id_type=MESH,
        )

    def norm_rows(x, gain):
        x32 = x.astype(F32)
        return x32 * lax.rsqrt(jnp.mean(x32 * x32, axis=-1, keepdims=True) + EPS) * gain

    gain = ng[...]
    for b in range(seqs):
        one = norm_rows(xd[pl.ds(b, 1), :], gain)
        nrm[pl.ds(rows + PAD * b, PAD), :] = jnp.broadcast_to(one, (PAD, one.shape[1])).astype(BF16)
    l_xp.wait()
    nrm[pl.ds(0, rows), :] = norm_rows(xp_v[...], gain).astype(BF16)
    l_wq.wait()
    q = jnp.dot(nrm[...], wq_v[...], preferred_element_type=F32).astype(BF16)
    qbuf[0] = q[:rows]
    pl.semaphore_wait(barrier, kv - 1 + tp - 1)
    for d in range(1, kv):
        q_copy(d).start()

    l_wk.wait()
    kn = jnp.dot(nrm[...], wk_v[...], preferred_element_type=F32).astype(BF16)
    l_wv.wait()
    vn = jnp.dot(nrm[...], wv_v[...], preferred_element_type=F32).astype(BF16)
    zeros = jnp.zeros((LANES - rows, width), BF16)
    for h in range(heads):
        knew[h, pl.ds(0, rows), :] = kn[:rows, h * width : (h + 1) * width]
        vnew[h, pl.ds(0, rows), :] = vn[:rows, h * width : (h + 1) * width]
        knew[h, pl.ds(rows, LANES - rows), :] = zeros
        vnew[h, pl.ds(rows, LANES - rows), :] = zeros

    l_ck.wait()
    l_cv.wait()
    head_gain = hg[...]

    def head_norm(att):
        return (
            att * lax.rsqrt(jnp.mean(att * att, axis=-1, keepdims=True) + EPS) * head_gain
        ).astype(BF16)

    slots = ck_v.shape[0] // seqs
    for b in range(seqs):
        first = rows + PAD * b
        row_head = iota((PAD, width), 0) // 2
        row_map = iota((PAD, width), 0) % 2
        lane_map = iota((PAD, width), 1) // half

        def pick(block):
            wide = block[first : first + PAD].astype(F32)
            out = wide[:, :width]
            for h in range(1, heads):
                out = jnp.where(row_head == h, wide[:, h * width : (h + 1) * width], out)
            return out

        q_rows = jnp.where(row_map == lane_map, pick(q), 0.0)
        s = dot_t(q_rows.astype(BF16), ck_v[pl.ds(b * slots, slots), :])
        key = iota(s.shape, 1)
        ok = (key // heads < ln[b]) & (key % heads == iota(s.shape, 0) // 2)
        s = jnp.where(ok, s, NEG)
        own = jnp.sum(q_rows * pick(kn), axis=-1, keepdims=True)
        top = jnp.maximum(jnp.max(s, axis=-1, keepdims=True), own)
        w = jnp.exp2((s - top) * scale)
        w_own = jnp.exp2((own - top) * scale)
        tot = jnp.sum(w, axis=-1, keepdims=True) + w_own
        mixed = jnp.dot(
            w.astype(BF16), cv_v[pl.ds(b * slots, slots), :], preferred_element_type=F32
        )
        mixed = (mixed + w_own.astype(BF16).astype(F32) * pick(vn)) / tot
        for h in range(heads):
            att = mixed[2 * h : 2 * h + 1] - lam[h] * mixed[2 * h + 1 : 2 * h + 2]
            hbuf[0, pl.ds(first, PAD), pl.ds(h * width, width)] = jnp.broadcast_to(
                head_norm(att), (PAD, width)
            )
    for d in range(1, tp):
        h_copy(d, rows, PAD * seqs, d_send, d_recv).start()

    l_pk.wait()
    kf[...] = pk_v[...].astype(F32)
    for h in range(heads):
        kh[h] = kf[pl.ds(h, cached, stride=heads), :].astype(BF16)
    l_pv.wait()
    vf[...] = pv_v[...].astype(F32)
    for h in range(heads):
        vh[h] = vf[pl.ds(h, cached, stride=heads), :].astype(BF16)

    span = group * rows
    lane_low = (iota((span, width), 1) < half).astype(F32)
    low = lane_low.astype(BF16)
    high = (1.0 - lane_low).astype(BF16)

    def attend(c):
        block = qbuf[pl.ds(c * group, group)].reshape(span, hw)
        place = iota((2 * span, LANES), 0) % span
        owner = place // rows + (me + c * group)
        owner = jnp.where(owner >= kv, owner - kv, owner)
        lane = iota((2 * span, LANES), 1)
        ok = (lane < rows) & (lane + me * rows <= owner * rows + place % rows)
        lane = iota((span, LANES), 1)
        kind = lane % (2 * maps)
        stats = jnp.zeros((span, LANES), F32)
        for h in range(heads):
            qh = block[:, h * width : (h + 1) * width]
            q2 = jnp.concatenate([qh * low, qh * high], axis=0)
            s1 = dot_t(q2, kh[h])
            s2 = jnp.where(ok, dot_t(q2, knew[h]), NEG)
            top = jnp.maximum(
                jnp.max(s1, axis=-1, keepdims=True), jnp.max(s2, axis=-1, keepdims=True)
            )
            w1 = jnp.exp2((s1 - top) * scale)
            w2 = jnp.exp2((s2 - top) * scale)
            tot = jnp.sum(w1, axis=-1, keepdims=True) + jnp.sum(w2, axis=-1, keepdims=True)
            mixed = jnp.dot(w1.astype(BF16), vh[h], preferred_element_type=F32) + jnp.dot(
                w2.astype(BF16), vnew[h], preferred_element_type=F32
            )
            mixed = mixed.astype(BF16)
            for m in range(2):
                at = 2 * h + m
                part = slice(m * span, (m + 1) * span)
                sbuf[pl.ds(c * group, group), pl.ds(at * rows, rows), :] = mixed[part].reshape(
                    group, rows, width
                )
                stats = jnp.where(kind == at, top[part], stats)
                stats = jnp.where(kind == maps + at, tot[part], stats)
        hi = stats.astype(BF16).astype(F32)
        rest = stats - hi
        mid = rest.astype(BF16).astype(F32)
        lo = rest - mid
        piece = lane // (2 * maps)
        packed = jnp.where(piece == 0, hi, jnp.where(piece == 1, mid, lo)).astype(BF16)
        sbuf[pl.ds(c * group, group), pl.ds(maps * rows, rows), :] = packed.reshape(
            group, rows, LANES
        )

    for d in range(1, kv):
        q_copy(d).wait_recv()
    chunks = kv // group
    if chunks == 1:
        attend(0)
    else:
        lax.fori_loop(0, chunks, lambda c, carry: (attend(c), carry)[1], 0)
    for d in range(1, kv):
        s_copy(d).start()
    rbuf[0] = sbuf[0]
    l_wo.wait()
    for d in range(1, kv):
        s_copy(d).wait_recv()

    stats = rbuf[:, pl.ds(maps * rows, rows), :].astype(F32).reshape(kv * rows, LANES)
    step = 2 * maps
    stats = stats + pltpu.roll(stats, LANES - step, 1) + pltpu.roll(stats, LANES - 2 * step, 1)
    tots = pltpu.roll(stats, LANES - maps, 1)
    top = stats[:rows]
    for p in range(1, kv):
        top = jnp.maximum(top, stats[p * rows : (p + 1) * rows])
    factors = []
    tot = jnp.zeros((rows, LANES), F32)
    for p in range(kv):
        part = slice(p * rows, (p + 1) * rows)
        factors.append(jnp.exp2((stats[part] - top) * scale))
        tot = tot + factors[p] * tots[part]
    lane = iota((rows, LANES), 1)
    sign = jnp.ones((rows, LANES), F32)
    for h in range(heads):
        sign = jnp.where(lane == 2 * h + 1, -lam[h], sign)
    inverse = sign / tot
    atts = [jnp.zeros((rows, width), F32) for _ in range(heads)]
    for p in range(kv):
        coef = factors[p] * inverse
        for at in range(maps):
            atts[at // 2] = atts[at // 2] + coef[:, at : at + 1] * rbuf[
                p, pl.ds(at * rows, rows), :
            ].astype(F32)
    for h in range(heads):
        hbuf[0, pl.ds(0, rows), pl.ds(h * width, width)] = head_norm(atts[h])
    for d in range(1, tp):
        h_copy(d, 0, rows, h_send, h_recv).start()

    def out_part(s):
        start = pl.multiple_of(lax.rem(col + s, tp) * hw, hw)
        return jnp.dot(hbuf[s], wo_v[pl.ds(start, hw), :], preferred_element_type=F32)

    acc = out_part(0)
    for d in range(1, tp):
        h_copy(tp - d, rows, PAD * seqs, d_send, d_recv).wait_recv()
        h_copy(tp - d, 0, rows, h_send, h_recv).wait_recv()
        acc = acc + out_part(d)
    po[...] = acc[:rows].astype(BF16)
    for b in range(seqs):
        do[pl.ds(b, 1), :] = acc[rows + PAD * b : rows + PAD * b + 1].astype(BF16)
    for d in range(1, kv):
        q_copy(d).wait_send()
        s_copy(d).wait_send()
    for d in range(1, tp):
        h_copy(d, rows, PAD * seqs, d_send, d_recv).wait_send()
        h_copy(d, 0, rows, h_send, h_recv).wait_send()


def shards(
    x_piece,
    x_decode,
    norm_gain,
    w_query,
    w_key,
    w_value,
    w_out,
    head_gain,
    lambdas,
    piece_keys,
    piece_values,
    cache_keys,
    cache_values,
    cache_lengths,
):
    rows, d_model = x_piece.shape
    seqs = x_decode.shape[0]
    heads = lambdas.shape[0]
    cached, _, width = piece_keys.shape
    slots = cache_keys.shape[1]
    kv = lax.axis_size("kv")
    tp = lax.axis_size("tp")
    hw = heads * width
    features = w_out.shape[1]
    total = rows + PAD * seqs
    group = max(1, min(kv, 128 // rows))
    any_spec = pl.BlockSpec(memory_space=pl.ANY)
    vmem = pl.BlockSpec(memory_space=pltpu.VMEM)
    smem = pl.BlockSpec(memory_space=pltpu.SMEM)
    dma = pltpu.SemaphoreType.DMA
    message = (2 * heads + 1) * rows
    scratch = [
        pltpu.VMEM((rows, d_model), BF16),
        pltpu.VMEM((d_model, hw), BF16),
        pltpu.VMEM((d_model, hw), BF16),
        pltpu.VMEM((d_model, hw), BF16),
        pltpu.VMEM(w_out.shape, BF16),
        pltpu.VMEM((cached * heads, width), BF16),
        pltpu.VMEM((cached * heads, width), BF16),
        pltpu.VMEM((seqs * slots * heads, width), BF16),
        pltpu.VMEM((seqs * slots * heads, width), BF16),
        pltpu.VMEM((total, d_model), BF16),
        pltpu.VMEM((cached * heads, width), F32),
        pltpu.VMEM((cached * heads, width), F32),
        pltpu.VMEM((heads, cached, width), BF16),
        pltpu.VMEM((heads, cached, width), BF16),
        pltpu.VMEM((heads, LANES, width), BF16),
        pltpu.VMEM((heads, LANES, width), BF16),
        pltpu.VMEM((kv, rows, hw), BF16),
        pltpu.VMEM((kv, message, width), BF16),
        pltpu.VMEM((kv, message, width), BF16),
        pltpu.VMEM((tp, total, hw), BF16),
        dma((9,)),
        dma((kv,)),
        dma((kv,)),
        dma((kv,)),
        dma((kv,)),
        dma((tp,)),
        dma((tp,)),
        dma((tp,)),
        dma((tp,)),
    ]
    return pl.pallas_call(
        functools.partial(step_kernel, kv, tp, rows, seqs, heads, width, group),
        out_shape=(
            jax.ShapeDtypeStruct((rows, features), BF16),
            jax.ShapeDtypeStruct((seqs, features), BF16),
        ),
        in_specs=[
            any_spec, vmem, vmem, any_spec, any_spec, any_spec, any_spec, vmem, smem,
            any_spec, any_spec, any_spec, any_spec, smem,
        ],
        out_specs=(vmem, vmem),
        scratch_shapes=scratch,
        compiler_params=pltpu.CompilerParams(collective_id=0, has_side_effects=True),
        name="step",
    )(
        x_piece,
        x_decode,
        norm_gain.reshape(1, d_model),
        w_query,
        w_key,
        w_value,
        w_out,
        head_gain.reshape(1, width),
        lambdas,
        piece_keys.reshape(cached * heads, width),
        piece_values.reshape(cached * heads, width),
        cache_keys.reshape(seqs * slots * heads, width),
        cache_values.reshape(seqs * slots * heads, width),
        cache_lengths,
    )


def solution(mesh):
    placed = (
        P("kv", None),
        P("kv", None),
        P(),
        P(None, "tp"),
        P(None, "tp"),
        P(None, "tp"),
        P(None, "tp"),
        P(),
        P("tp"),
        P("kv", "tp", None),
        P("kv", "tp", None),
        P("kv", None, "tp", None),
        P("kv", None, "tp", None),
        P("kv"),
    )
    return jax.shard_map(
        shards,
        mesh=mesh,
        in_specs=placed,
        out_specs=(P("kv", "tp"), P("kv", "tp")),
        check_vma=False,
    )
```

time: 113 us -> 24.7 us (0.22)
  blocking collectives: 37.7 us -> 0 us
  waiting for transfers between devices: 28.8 us -> 0 us
  starting transfers between devices: 25 us -> 0 us
  Pallas kernels: 0 us -> 21.3 us
  local copies, waits for them, and re-layouts: 11.4 us -> 1.91 us
  matrix products: 4.9 us -> 0 us
  other arithmetic: 2.63 us -> 0 us
    all_gather x2 -> x0, blocking collectives: 37.7 us -> none  [the longest x1 32.5 us: shards(): piece = lax.all_gather(queries[:piece_rows], 'kv', axis=0, tiled=True)]
    all_to_all x6 -> x0, waiting for transfers between devices: 28.8 us -> none  [the longest x1 6.8 us: shards(): lax.all_to_all(partials[2].astype(jnp.bfloat16), 'kv', split_axis=0, conc...]
    all_to_all x6 -> x0, starting transfers between devices: 25 us -> none  [the longest x1 6.13 us: shards(): lax.all_to_all(partials[3], 'kv', split_axis=1, concat_axis=1, tiled=True)]
    pallas_call x0 -> x1, Pallas kernels: none -> 21.3 us  [shards(): pl.pallas_call(functools.partial(step_kernel, kv, tp, rows, seqs, heads,...]
    dot_general x12 -> x0, matrix products: 4.9 us -> none  [the longest x1 1.56 us: shards(): jnp.dot(normed, w_query, preferred_element_type=jnp.float32)]
    all_to_all x8 -> x0, local copies, waits for them, and re-layouts: 2.74 us -> none  [the longest x2 0.69 us: shards(): lax.all_to_all(partials[4], 'kv', split_axis=1, concat_axis=1, tiled=True)]
    another operation x2 -> x0, local copies, waits for them, and re-layouts: 1.97 us -> none
    reduce_sum x9 -> x0, other arithmetic: 1.75 us -> none  [the longest x1 1.14 us: shards(): jnp.mean(rows32 * rows32, axis=-1, keepdims=True) + EPS]
  transfers between devices with their start and end apart: 6 -> 0, of which waited for: 5 -> 0; matrix products, arithmetic and copies ran while one was open for 9% -> 0% of each run, Pallas kernels for 0% -> 0%
where the time goes in v1:
time: 24.7 us; the launch traced here: 24.5 us
  Pallas kernels  21.3 us (86%)
  local copies, waits for them, and re-layouts  1.91 us (8%)
  between operations  1.3 us (5%)
    pallas_call x1, Pallas kernels, shards(): pl.pallas_call(functools.partial(step_kernel, kv, tp, rows, seqs, heads,...  21.3 us
    unnamed x4, local copies, waits for them, and re-layouts  1.91 us

profile of v1, /device:TPU:0, one launch (start us, length us, event | category | flops | bytes accessed | tf_op | source)
XLA Modules:
  0.0 24.5 jit_solution(14292231932300565050)
XLA Ops:
  1.3 21.3 %step.1 = (bf16[16,512]{1,0:T(8,128)(2,1)}, bf16[1,512]{1,0:T(2,128)(2,1)}) custom-call(bf16[16,2048]{1,0:T(8,128)(2,1)} %xp.1, bf16[1,2048]{1,0:T(2,128)(2,1)} %xd.1, f32[1,2048]{1,0:T(1,128)} %bitcast.10, bf16[2048,256]{1,0:T(8,128)(2,1)} %wq.1, bf16[2048,256]{1,0:T(8,128)(2,1)} %wk.1, bf16[2048,256]{1,0:T(8,128)(2,1)} %wv.1, bf16[1024,512]{1,0:T(8,128)(2,1)} %wo.1, ...), custom_call_target="tpu_custom_call" | custom-call | tf_op jit(solution)/shard_map/step/pallas_call | solution.py:344
  22.5 0.0 copy-start
  22.6 1.3 %copy.19 = bf16[16,512]{1,0:T(8,128)(2,1)} copy(bf16[16,512]{1,0:T(8,128)(2,1)} %get-tuple-element.4) | data formatting | bytes 32768
  23.9 0.0 copy-done
  23.9 0.6 %copy.20 = bf16[1,512]{1,0:T(2,128)(2,1)} copy(bf16[1,512]{1,0:T(2,128)(2,1)S(1)} %copy-done) | data formatting | bytes 2048
Async XLA Ops:
  22.5 1.3 %copy-start = (bf16[1,512]{1,0:T(2,128)(2,1)S(1)}, bf16[1,512]{1,0:T(2,128)(2,1)}, u32[]{:S(2)}) copy-start(bf16[1,512]{1,0:T(2,128)(2,1)} %get-tuple-element.5) | copy-start | bytes 3076

commit v2 on v1

--- a/solution.py
+++ b/solution.py
@@ -29,7 +29,7 @@
     kv, tp, rows, seqs, heads, width, group,
     xp, xd, ng, wq, wk, wv, wo, hg, lam, pk, pv, ck, cv, ln,
     po, do,
-    xp_v, wq_v, wk_v, wv_v, wo_v, pk_v, pv_v, ck_v, cv_v,
+    xp_v, xd_v, ng_v, hg_v, lam_s, ln_s, wq_v, wk_v, wv_v, wo_v, pk_v, pv_v, ck_v, cv_v,
     nrm, kf, vf, kh, vh, knew, vnew, qbuf, sbuf, rbuf, hbuf,
     load_sem, q_send, q_recv, s_send, s_recv, d_send, d_recv, h_send, h_recv,
 ):
@@ -39,41 +39,58 @@
     scale = math.log2(math.e) / math.sqrt(half)
     me = lax.axis_index("kv")
     col = lax.axis_index("tp")
-    total = rows + PAD * seqs
     cached = kh.shape[1]
 
     pairs = [
-        (xp, xp_v), (wq, wq_v), (wk, wk_v), (wv, wv_v), (ck, ck_v), (cv, cv_v),
-        (pk, pk_v), (pv, pv_v), (wo, wo_v),
+        (xp, xp_v), (ng, ng_v), (xd, xd_v), (wq, wq_v), (lam, lam_s), (ln, ln_s), (hg, hg_v),
+        (wk, wk_v), (wv, wv_v), (ck, ck_v), (cv, cv_v), (pk, pk_v), (pv, pv_v), (wo, wo_v),
     ]
     loads = [pltpu.make_async_copy(s, d, load_sem.at[i]) for i, (s, d) in enumerate(pairs)]
     for load in loads:
         load.start()
-    l_xp, l_wq, l_wk, l_wv, l_ck, l_cv, l_pk, l_pv, l_wo = loads
+    l_xp, l_ng, l_xd, l_wq, l_lam, l_ln, l_hg, l_wk, l_wv, l_ck, l_cv, l_pk, l_pv, l_wo = loads
+
+    bits = kv.bit_length() - 1
+    paired = kv == 1 << bits
+
+    def partner(d):
+        if not paired:
+            return lax.rem(me + d, kv)
+        out = 0
+        for b in range(bits):
+            mine = lax.rem(lax.div(me, 1 << b), 2)
+            if isinstance(d, int):
+                out = out + (1 << b) * ((1 - mine) if (d >> b) & 1 else mine)
+            else:
+                out = out + (1 << b) * lax.rem(mine + lax.rem(lax.div(d, 1 << b), 2), 2)
+        return out
 
     def kv_peer(d):
-        return {"kv": lax.rem(me + d, kv)}
+        return {"kv": partner(d)}
+
+    def back(d):
+        return d if paired else kv - d
 
     def tp_peer(d):
         return {"tp": lax.rem(col + d, tp)}
 
     barrier = pltpu.get_barrier_semaphore()
-    for d in range(1, kv):
+    for d in range(kv - 1, 0, -1):
         pl.semaphore_signal(barrier, inc=1, device_id=kv_peer(d), device_id_type=MESH)
     for d in range(1, tp):
         pl.semaphore_signal(barrier, inc=1, device_id=tp_peer(d), device_id_type=MESH)
 
     def q_copy(d):
         return pltpu.make_async_remote_copy(
-            src_ref=qbuf.at[0], dst_ref=qbuf.at[kv - d],
-            send_sem=q_send.at[d], recv_sem=q_recv.at[kv - d],
+            src_ref=qbuf.at[0], dst_ref=qbuf.at[back(d)],
+            send_sem=q_send.at[d], recv_sem=q_recv.at[back(d)],
             device_id=kv_peer(d), device_id_type=MESH,
         )
 
     def s_copy(d):
         return pltpu.make_async_remote_copy(
-            src_ref=sbuf.at[d], dst_ref=rbuf.at[kv - d],
-            send_sem=s_send.at[d], recv_sem=s_recv.at[kv - d],
+            src_ref=sbuf.at[d], dst_ref=rbuf.at[back(d)],
+            send_sem=s_send.at[d], recv_sem=s_recv.at[back(d)],
             device_id=kv_peer(d), device_id_type=MESH,
         )
 
@@ -88,17 +105,19 @@
         x32 = x.astype(F32)
         return x32 * lax.rsqrt(jnp.mean(x32 * x32, axis=-1, keepdims=True) + EPS) * gain
 
-    gain = ng[...]
+    l_xp.wait()
+    l_ng.wait()
+    gain = ng_v[...]
+    nrm[pl.ds(0, rows), :] = norm_rows(xp_v[...], gain).astype(BF16)
+    l_xd.wait()
     for b in range(seqs):
-        one = norm_rows(xd[pl.ds(b, 1), :], gain)
+        one = norm_rows(xd_v[pl.ds(b, 1), :], gain)
         nrm[pl.ds(rows + PAD * b, PAD), :] = jnp.broadcast_to(one, (PAD, one.shape[1])).astype(BF16)
-    l_xp.wait()
-    nrm[pl.ds(0, rows), :] = norm_rows(xp_v[...], gain).astype(BF16)
     l_wq.wait()
     q = jnp.dot(nrm[...], wq_v[...], preferred_element_type=F32).astype(BF16)
     qbuf[0] = q[:rows]
     pl.semaphore_wait(barrier, kv - 1 + tp - 1)
-    for d in range(1, kv):
+    for d in range(kv - 1, 0, -1):
         q_copy(d).start()
 
     l_wk.wait()
@@ -114,7 +133,10 @@
 
     l_ck.wait()
     l_cv.wait()
-    head_gain = hg[...]
+    l_hg.wait()
+    l_lam.wait()
+    l_ln.wait()
+    head_gain = hg_v[...]
 
     def head_norm(att):
         return (
@@ -138,7 +160,7 @@
         q_rows = jnp.where(row_map == lane_map, pick(q), 0.0)
         s = dot_t(q_rows.astype(BF16), ck_v[pl.ds(b * slots, slots), :])
         key = iota(s.shape, 1)
-        ok = (key // heads < ln[b]) & (key % heads == iota(s.shape, 0) // 2)
+        ok = (key // heads < ln_s[b]) & (key % heads == iota(s.shape, 0) // 2)
         s = jnp.where(ok, s, NEG)
         own = jnp.sum(q_rows * pick(kn), axis=-1, keepdims=True)
         top = jnp.maximum(jnp.max(s, axis=-1, keepdims=True), own)
@@ -150,7 +172,7 @@
         )
         mixed = (mixed + w_own.astype(BF16).astype(F32) * pick(vn)) / tot
         for h in range(heads):
-            att = mixed[2 * h : 2 * h + 1] - lam[h] * mixed[2 * h + 1 : 2 * h + 2]
+            att = mixed[2 * h : 2 * h + 1] - lam_s[h] * mixed[2 * h + 1 : 2 * h + 2]
             hbuf[0, pl.ds(first, PAD), pl.ds(h * width, width)] = jnp.broadcast_to(
                 head_norm(att), (PAD, width)
             )
@@ -174,10 +196,12 @@
     def attend(c):
         block = qbuf[pl.ds(c * group, group)].reshape(span, hw)
         place = iota((2 * span, LANES), 0) % span
-        owner = place // rows + (me + c * group)
-        owner = jnp.where(owner >= kv, owner - kv, owner)
+        slot = place // rows
+        ahead = place % rows
+        for g in range(group):
+            ahead = jnp.where(slot == g, ahead + (partner(c * group + g) - me) * rows, ahead)
         lane = iota((2 * span, LANES), 1)
-        ok = (lane < rows) & (lane + me * rows <= owner * rows + place % rows)
+        ok = (lane < rows) & (lane <= ahead)
         lane = iota((span, LANES), 1)
         kind = lane % (2 * maps)
         stats = jnp.zeros((span, LANES), F32)
@@ -214,15 +238,21 @@
             group, rows, LANES
         )
 
-    for d in range(1, kv):
-        q_copy(d).wait_recv()
     chunks = kv // group
-    if chunks == 1:
-        attend(0)
+    if chunks <= 2:
+        for c in range(chunks):
+            members = range(max(1, c * group), (c + 1) * group)
+            for d in members:
+                q_copy(d).wait_recv()
+            attend(c)
+            for d in members:
+                s_copy(d).start()
     else:
+        for d in range(1, kv):
+            q_copy(d).wait_recv()
         lax.fori_loop(0, chunks, lambda c, carry: (attend(c), carry)[1], 0)
-    for d in range(1, kv):
-        s_copy(d).start()
+        for d in range(1, kv):
+            s_copy(d).start()
     rbuf[0] = sbuf[0]
     l_wo.wait()
     for d in range(1, kv):
@@ -244,7 +274,7 @@
     lane = iota((rows, LANES), 1)
     sign = jnp.ones((rows, LANES), F32)
     for h in range(heads):
-        sign = jnp.where(lane == 2 * h + 1, -lam[h], sign)
+        sign = jnp.where(lane == 2 * h + 1, -lam_s[h], sign)
     inverse = sign / tot
     atts = [jnp.zeros((rows, width), F32) for _ in range(heads)]
     for p in range(kv):
@@ -304,14 +334,18 @@
     hw = heads * width
     features = w_out.shape[1]
     total = rows + PAD * seqs
-    group = max(1, min(kv, 128 // rows))
-    any_spec = pl.BlockSpec(memory_space=pl.ANY)
+    group = max(1, min(kv // 2, 128 // rows))
+    hbm = pl.BlockSpec(memory_space=pltpu.HBM)
     vmem = pl.BlockSpec(memory_space=pltpu.VMEM)
-    smem = pl.BlockSpec(memory_space=pltpu.SMEM)
     dma = pltpu.SemaphoreType.DMA
     message = (2 * heads + 1) * rows
     scratch = [
         pltpu.VMEM((rows, d_model), BF16),
+        pltpu.VMEM((seqs, d_model), BF16),
+        pltpu.VMEM((1, d_model), F32),
+        pltpu.VMEM((1, width), F32),
+        pltpu.SMEM((heads,), F32),
+        pltpu.SMEM((seqs,), jnp.int32),
         pltpu.VMEM((d_model, hw), BF16),
         pltpu.VMEM((d_model, hw), BF16),
         pltpu.VMEM((d_model, hw), BF16),
@@ -331,7 +365,7 @@
         pltpu.VMEM((kv, message, width), BF16),
         pltpu.VMEM((kv, message, width), BF16),
         pltpu.VMEM((tp, total, hw), BF16),
-        dma((9,)),
+        dma((14,)),
         dma((kv,)),
         dma((kv,)),
         dma((kv,)),
@@ -344,13 +378,10 @@
     return pl.pallas_call(
         functools.partial(step_kernel, kv, tp, rows, seqs, heads, width, group),
         out_shape=(
-            jax.ShapeDtypeStruct((rows, features), BF16),
-            jax.ShapeDtypeStruct((seqs, features), BF16),
+            pltpu.VMEM((rows, features), BF16),
+            pltpu.VMEM((seqs, features), BF16),
         ),
-        in_specs=[
-            any_spec, vmem, vmem, any_spec, any_spec, any_spec, any_spec, vmem, smem,
-            any_spec, any_spec, any_spec, any_spec, smem,
-        ],
+        in_specs=[hbm] * 14,
         out_specs=(vmem, vmem),
         scratch_shapes=scratch,
         compiler_params=pltpu.CompilerParams(collective_id=0, has_side_effects=True),

time: 24.7 us -> 22.7 us (0.919)
  Pallas kernels: 21.3 us -> 20 us
  local copies, waits for them, and re-layouts: 1.91 us -> 1.19 us
    pallas_call x1, Pallas kernels: 21.3 us -> 20 us  [shards(): pl.pallas_call(functools.partial(step_kernel, kv, tp, rows, seqs, heads,...]
    unnamed x4 -> x2, local copies, waits for them, and re-layouts: 1.91 us -> 1.19 us
where the time goes in v2:
time: 22.7 us; the launch traced here: 22.5 us
  Pallas kernels  20 us (88%)
  between operations  1.29 us (6%)
  local copies, waits for them, and re-layouts  1.19 us (5%)
    pallas_call x1, Pallas kernels, shards(): pl.pallas_call(functools.partial(step_kernel, kv, tp, rows, seqs, heads,...  20 us
    unnamed x2, local copies, waits for them, and re-layouts  1.19 us

profile of v2, /device:TPU:0, one launch (start us, length us, event | category | flops | bytes accessed | tf_op | source)
XLA Modules:
  0.0 22.5 jit_solution(11471987846492996841)
XLA Ops:
  1.3 20.0 %step.1 = (bf16[16,512]{1,0:T(8,128)(2,1)S(1)}, bf16[1,512]{1,0:T(2,128)(2,1)S(1)}) custom-call(bf16[16,2048]{1,0:T(8,128)(2,1)} %xp.1, bf16[1,2048]{1,0:T(2,128)(2,1)} %xd.1, f32[1,2048]{1,0:T(1,128)} %bitcast.10, bf16[2048,256]{1,0:T(8,128)(2,1)} %wq.1, bf16[2048,256]{1,0:T(8,128)(2,1)} %wk.1, bf16[2048,256]{1,0:T(8,128)(2,1)} %wv.1, ...), custom_call_target="tpu_custom_call" | custom-call | tf_op jit(solution)/shard_map/step/pallas_call | solution.py:378
  21.3 0.6 %copy.18 = bf16[16,512]{1,0:T(8,128)(2,1)} copy(bf16[16,512]{1,0:T(8,128)(2,1)S(1)} %get-tuple-element.2) | data formatting | bytes 32768
  21.9 0.6 %copy.19 = bf16[1,512]{1,0:T(2,128)(2,1)} copy(bf16[1,512]{1,0:T(2,128)(2,1)S(1)} %get-tuple-element.3) | data formatting | bytes 2048

commit v3 on v2

--- a/solution.py
+++ b/solution.py
@@ -46,7 +46,7 @@
         (wk, wk_v), (wv, wv_v), (ck, ck_v), (cv, cv_v), (pk, pk_v), (pv, pv_v), (wo, wo_v),
     ]
     loads = [pltpu.make_async_copy(s, d, load_sem.at[i]) for i, (s, d) in enumerate(pairs)]
-    for load in loads:
+    for load in loads[:4]:
         load.start()
     l_xp, l_ng, l_xd, l_wq, l_lam, l_ln, l_hg, l_wk, l_wv, l_ck, l_cv, l_pk, l_pv, l_wo = loads
 
@@ -87,9 +87,12 @@
             device_id=kv_peer(d), device_id_type=MESH,
         )
 
-    def s_copy(d):
+    message = sbuf.shape[1]
+
+    def s_copy(d, start=0, size=message):
         return pltpu.make_async_remote_copy(
-            src_ref=sbuf.at[d], dst_ref=rbuf.at[back(d)],
+            src_ref=sbuf.at[d, pl.ds(start, size)],
+            dst_ref=rbuf.at[back(d), pl.ds(start, size)],
             send_sem=s_send.at[d], recv_sem=s_recv.at[back(d)],
             device_id=kv_peer(d), device_id_type=MESH,
         )
@@ -106,6 +109,8 @@
         return x32 * lax.rsqrt(jnp.mean(x32 * x32, axis=-1, keepdims=True) + EPS) * gain
 
     l_xp.wait()
+    for load in loads[4:]:
+        load.start()
     l_ng.wait()
     gain = ng_v[...]
     nrm[pl.ds(0, rows), :] = norm_rows(xp_v[...], gain).astype(BF16)
@@ -193,7 +198,7 @@
     low = lane_low.astype(BF16)
     high = (1.0 - lane_low).astype(BF16)
 
-    def attend(c):
+    def attend(c, members=()):
         block = qbuf[pl.ds(c * group, group)].reshape(span, hw)
         place = iota((2 * span, LANES), 0) % span
         slot = place // rows
@@ -228,6 +233,9 @@
                 )
                 stats = jnp.where(kind == at, top[part], stats)
                 stats = jnp.where(kind == maps + at, tot[part], stats)
+            if h < heads - 1:
+                for d in members:
+                    s_copy(d, 2 * h * rows, 2 * rows).start()
         hi = stats.astype(BF16).astype(F32)
         rest = stats - hi
         mid = rest.astype(BF16).astype(F32)
@@ -237,16 +245,16 @@
         sbuf[pl.ds(c * group, group), pl.ds(maps * rows, rows), :] = packed.reshape(
             group, rows, LANES
         )
+        for d in members:
+            s_copy(d, 2 * (heads - 1) * rows, 3 * rows).start()
 
     chunks = kv // group
     if chunks <= 2:
         for c in range(chunks):
-            members = range(max(1, c * group), (c + 1) * group)
+            members = range((c + 1) * group - 1, max(1, c * group) - 1, -1)
             for d in members:
                 q_copy(d).wait_recv()
-            attend(c)
-            for d in members:
-                s_copy(d).start()
+            attend(c, members)
     else:
         for d in range(1, kv):
             q_copy(d).wait_recv()
@@ -306,6 +314,14 @@
     for d in range(1, tp):
         h_copy(d, rows, PAD * seqs, d_send, d_recv).wait_send()
         h_copy(d, 0, rows, h_send, h_recv).wait_send()
+
+
+def store_kernel(a, b, po, do, sem):
+    copies = [pltpu.make_async_copy(a, po, sem.at[0]), pltpu.make_async_copy(b, do, sem.at[1])]
+    for copy in copies:
+        copy.start()
+    for copy in copies:
+        copy.wait()
 
 
 def shards(
@@ -375,7 +391,7 @@
         dma((tp,)),
         dma((tp,)),
     ]
-    return pl.pallas_call(
+    held = pl.pallas_call(
         functools.partial(step_kernel, kv, tp, rows, seqs, heads, width, group),
         out_shape=(
             pltpu.VMEM((rows, features), BF16),
@@ -402,6 +418,14 @@
         cache_values.reshape(seqs * slots * heads, width),
         cache_lengths,
     )
+    return pl.pallas_call(
+        store_kernel,
+        out_shape=tuple(jax.ShapeDtypeStruct(a.shape, a.dtype) for a in held),
+        in_specs=[vmem, vmem],
+        out_specs=(hbm, hbm),
+        scratch_shapes=[dma((2,))],
+        name="store",
+    )(*[pltpu.with_memory_space_constraint(a, pltpu.VMEM) for a in held])
 
 
 def solution(mesh):

time: 22.7 us -> 21.9 us (0.965)
  local copies, waits for them, and re-layouts: 1.19 us -> 0 us
  Pallas kernels: 20 us -> 20.4 us
    unnamed x2 -> x0, local copies, waits for them, and re-layouts: 1.19 us -> none
    pallas_call x0 -> x1, Pallas kernels: none -> 0.63 us  [shards(): pl.pallas_call(store_kernel, out_shape=tuple((jax.ShapeDtypeStruct(a.shap...]
    pallas_call x1, Pallas kernels: 20 us -> 19.8 us  [shards(): pl.pallas_call(functools.partial(step_kernel, kv, tp, rows, seqs, heads,...]
where the time goes in v3:
time: 21.9 us; the launch traced here: 21.7 us
  Pallas kernels  20.4 us (93%)
  between operations  1.29 us (6%)
    pallas_call x1, Pallas kernels, shards(): pl.pallas_call(functools.partial(step_kernel, kv, tp, rows, seqs, heads,...  19.8 us
    pallas_call x1, Pallas kernels, shards(): pl.pallas_call(store_kernel, out_shape=tuple((jax.ShapeDtypeStruct(a.shap...  0.63 us

profile of v3, /device:TPU:0, one launch (start us, length us, event | category | flops | bytes accessed | tf_op | source)
XLA Modules:
  0.0 21.7 jit_solution(9353747673522673298)
XLA Ops:
  1.3 19.8 %step.1 = (bf16[16,512]{1,0:T(8,128)(2,1)S(1)}, bf16[1,512]{1,0:T(2,128)(2,1)S(1)}) custom-call(bf16[16,2048]{1,0:T(8,128)(2,1)} %xp.1, bf16[1,2048]{1,0:T(2,128)(2,1)} %xd.1, f32[1,2048]{1,0:T(1,128)} %bitcast.10, bf16[2048,256]{1,0:T(8,128)(2,1)} %wq.1, bf16[2048,256]{1,0:T(8,128)(2,1)} %wk.1, bf16[2048,256]{1,0:T(8,128)(2,1)} %wv.1, ...), custom_call_target="tpu_custom_call" | custom-call | tf_op jit(solution)/shard_map/step/pallas_call | solution.py:394
  21.1 0.6 %store.1 = (bf16[16,512]{1,0:T(8,128)(2,1)}, bf16[1,512]{1,0:T(2,128)(2,1)}) custom-call(bf16[16,512]{1,0:T(8,128)(2,1)S(1)} %get-tuple-element.4.a, bf16[1,512]{1,0:T(2,128)(2,1)S(1)} %get-tuple-element.5.b), custom_call_target="tpu_custom_call" | custom-call | tf_op jit(solution)/shard_map/store/pallas_call | solution.py:421

commit v4 on v3

--- a/solution.py
+++ b/solution.py
@@ -88,6 +88,7 @@
         )
 
     message = sbuf.shape[1]
+    fold = rows // 2
 
     def s_copy(d, start=0, size=message):
         return pltpu.make_async_remote_copy(
@@ -241,12 +242,14 @@
         mid = rest.astype(BF16).astype(F32)
         lo = rest - mid
         piece = lane // (2 * maps)
-        packed = jnp.where(piece == 0, hi, jnp.where(piece == 1, mid, lo)).astype(BF16)
-        sbuf[pl.ds(c * group, group), pl.ds(maps * rows, rows), :] = packed.reshape(
-            group, rows, LANES
-        )
+        packed = jnp.where(piece == 0, hi, jnp.where(piece == 1, mid, lo))
+        packed = jnp.where(piece < 3, packed, 0.0).reshape(group, 2, fold, LANES)
+        upper = pltpu.roll(packed[:, 1].reshape(group * fold, LANES), LANES // 2, 1)
+        sbuf[pl.ds(c * group, group), pl.ds(maps * rows, fold), :] = (
+            packed[:, 0] + upper.reshape(group, fold, LANES)
+        ).astype(BF16)
         for d in members:
-            s_copy(d, 2 * (heads - 1) * rows, 3 * rows).start()
+            s_copy(d, 2 * (heads - 1) * rows, 2 * rows + fold).start()
 
     chunks = kv // group
     if chunks <= 2:
@@ -266,7 +269,10 @@
     for d in range(1, kv):
         s_copy(d).wait_recv()
 
-    stats = rbuf[:, pl.ds(maps * rows, rows), :].astype(F32).reshape(kv * rows, LANES)
+    lower = rbuf[:, pl.ds(maps * rows, fold), :].astype(F32)
+    upper = pltpu.roll(lower.reshape(kv * fold, LANES), LANES // 2, 1)
+    stats = jnp.concatenate([lower, upper.reshape(kv, fold, LANES)], axis=1)
+    stats = stats.reshape(kv * rows, LANES)
     step = 2 * maps
     stats = stats + pltpu.roll(stats, LANES - step, 1) + pltpu.roll(stats, LANES - 2 * step, 1)
     tots = pltpu.roll(stats, LANES - maps, 1)
@@ -354,7 +360,7 @@
     hbm = pl.BlockSpec(memory_space=pltpu.HBM)
     vmem = pl.BlockSpec(memory_space=pltpu.VMEM)
     dma = pltpu.SemaphoreType.DMA
-    message = (2 * heads + 1) * rows
+    message = 2 * heads * rows + rows // 2
     scratch = [
         pltpu.VMEM((rows, d_model), BF16),
         pltpu.VMEM((seqs, d_model), BF16),

time: 21.9 us -> 21.5 us (0.982)
  Pallas kernels: 20.4 us -> 20.1 us
    pallas_call x1, Pallas kernels: 19.8 us -> 19.4 us  [shards(): pl.pallas_call(functools.partial(step_kernel, kv, tp, rows, seqs, heads,...]
where the time goes in v4:
time: 21.5 us; the launch traced here: 21.4 us
  Pallas kernels  20.1 us (93%)
  between operations  1.29 us (6%)
    pallas_call x1, Pallas kernels, shards(): pl.pallas_call(functools.partial(step_kernel, kv, tp, rows, seqs, heads,...  19.4 us
    pallas_call x1, Pallas kernels, shards(): pl.pallas_call(store_kernel, out_shape=tuple((jax.ShapeDtypeStruct(a.shap...  0.63 us

profile of v4, /device:TPU:0, one launch (start us, length us, event | category | flops | bytes accessed | tf_op | source)
XLA Modules:
  0.0 21.4 jit_solution(11969387862921358248)
XLA Ops:
  1.3 19.4 %step.1 = (bf16[16,512]{1,0:T(8,128)(2,1)S(1)}, bf16[1,512]{1,0:T(2,128)(2,1)S(1)}) custom-call(bf16[16,2048]{1,0:T(8,128)(2,1)} %xp.1, bf16[1,2048]{1,0:T(2,128)(2,1)} %xd.1, f32[1,2048]{1,0:T(1,128)} %bitcast.10, bf16[2048,256]{1,0:T(8,128)(2,1)} %wq.1, bf16[2048,256]{1,0:T(8,128)(2,1)} %wk.1, bf16[2048,256]{1,0:T(8,128)(2,1)} %wv.1, ...), custom_call_target="tpu_custom_call" | custom-call | tf_op jit(solution)/shard_map/step/pallas_call | solution.py:400
  20.7 0.6 %store.1 = (bf16[16,512]{1,0:T(8,128)(2,1)}, bf16[1,512]{1,0:T(2,128)(2,1)}) custom-call(bf16[16,512]{1,0:T(8,128)(2,1)S(1)} %get-tuple-element.4.a, bf16[1,512]{1,0:T(2,128)(2,1)S(1)} %get-tuple-element.5.b), custom_call_target="tpu_custom_call" | custom-call | tf_op jit(solution)/shard_map/store/pallas_call | solution.py:427
